TPU v7x, 128 devices: a whole 4x4x4 slice. The times are simulated.
128 devices in a mesh: rep: 16 (over z, x), fs: 4 (over y), tp: 2 (over core).
Axes of the slice: x: 4, y: 4, z: 4, core: 2. Of those that a mesh axis runs over, the one named last changes fastest.
Arguments:
- inputs: bfloat16 [16384, 2048], P(('rep', 'fs', 'tp')), may hold values from -6 to 6
- out_grad: bfloat16 [16384, 2048], P(('rep', 'fs', 'tp')), may hold values from -24 to 24
- pre_act: bfloat16 [16384, 8192], P('rep', ('fs', 'tp')), may hold values from -6 to 6
- w_up: bfloat16 [2048, 8192], P('rep', ('fs', 'tp')), may hold values from -0.125 to 0.125
- w_down_t: bfloat16 [2048, 8192], P('rep', ('fs', 'tp')), may hold values from -0.0625 to 0.0625
Outputs:
- grad_in: bfloat16 [16384, 2048], P(('rep', 'fs', 'tp'))
- grad_up: float32 [2048, 8192], P('rep', ('fs', 'tp'))
- grad_down_t: float32 [2048, 8192], P('rep', ('fs', 'tp'))
All inputs are finite; a program needn't handle non-finite values.
Results may differ from a plain program's by a relative error of at most 0.014.
Values may be sent and summed in bfloat16 or wider, within the bound.
A program may use at most 128 MiB of HBM per device.

v0:
```python
import jax
import jax.numpy as jnp
from jax import lax
from jax.sharding import PartitionSpec as P


def side_by_side(arrays, axis, dim, along):
    widths = [a.shape[along] for a in arrays]
    both = jnp.concatenate(arrays, axis=along)
    out = lax.all_gather(both, axis, axis=dim, tiled=True)
    return tuple(jnp.split(out, [sum(widths[:k]) for k in range(1, len(widths))], axis=along))


def cut_along(shard, dim, length):
    shape = shard.shape
    tiles = shard.reshape(*shape[:dim], length, shape[dim] // length, *shape[dim + 1 :])
    return jnp.moveaxis(tiles, dim, 0)


def sent_and_summed(shard, axis, dim):
    tiles = cut_along(shard, dim, lax.axis_size(axis))
    arrived = lax.all_to_all(tiles, axis, split_axis=0, concat_axis=0, tiled=True)
    return arrived.astype(jnp.float32).sum(axis=0)


def on_device(inputs, out_grad, pre_act, w_up, w_down_t):
    input_rows, grad_rows = side_by_side((inputs, out_grad), ("fs", "tp"), 0, 1)
    row_count, col_count = pre_act.shape
    pre_float = pre_act.astype(jnp.float32)
    linear = jnp.maximum(pre_float, 0.0)
    squared = (linear * linear).astype(jnp.bfloat16)
    grad_squared = jnp.dot(
        grad_rows,
        lax.all_gather(w_down_t, "rep", axis=0, tiled=True),
        preferred_element_type=jnp.float32,
    )
    grad_pre = (grad_squared * 2.0 * linear).astype(jnp.bfloat16)
    partial_terms = lax.dot_general(
        grad_pre,
        lax.all_gather(w_up, "rep", axis=0, tiled=True),
        (((1,), (1,)), ((), ())),
        preferred_element_type=jnp.float32,
    ).astype(jnp.bfloat16)
    grad_in = sent_and_summed(
        partial_terms.astype(jnp.float32).astype(jnp.bfloat16), ("fs", "tp"), 0
    ).astype(jnp.bfloat16)
    total_tokens = row_count * lax.axis_size("rep")
    factor = float(total_tokens) ** (-0.5)
    down_part = lax.dot_general(
        grad_rows, squared, (((0,), (0,)), ((), ())), preferred_element_type=jnp.float32
    )
    up_part = lax.dot_general(
        input_rows, grad_pre, (((0,), (0,)), ((), ())), preferred_element_type=jnp.float32
    )
    stacked = lax.psum_scatter(
        (jnp.concatenate([down_part, up_part], axis=1) * factor).astype(jnp.bfloat16),
        "rep",
        scatter_dimension=0,
        tiled=True,
    ).astype(jnp.float32)
    grad_down_t = stacked[:, :col_count]
    grad_up = stacked[:, col_count:]
    return (grad_in, grad_up, grad_down_t)


def solution(mesh):
    in_specs = (
        P(("rep", "fs", "tp"), None),
        P(("rep", "fs", "tp"), None),
        P("rep", ("fs", "tp")),
        P("rep", ("fs", "tp")),
        P("rep", ("fs", "tp")),
    )
    out_specs = (P(("rep", "fs", "tp"), None), P("rep", ("fs", "tp")), P("rep", ("fs", "tp")))
    return jax.shard_map(
        on_device, mesh=mesh, in_specs=in_specs, out_specs=out_specs, check_vma=False
    )
```

profile of v0, /device:TPU:0, one launch (start us, length us, event | category | flops | bytes accessed | tf_op | source)
XLA Modules:
  0.0 267.7 jit_solution(14350902395174839867)
XLA Ops:
  7.2 0.0 all-gather.4.cloned.1.call-start
  7.2 2.4 pad_maximum_fusion
  9.6 0.0 all-gather.6.cloned.1.call-start
  9.6 0.7 all-gather.6.cloned.1.call-update
  10.3 0.0 all-gather.8.cloned.1.call-start
  10.4 0.7 all-gather.8.cloned.1.call-update
  11.1 0.0 reduce-scatter.4.cloned.1.call-start
  11.1 50.8 %all-gather.4.cloned.1.call-done = bf16[1024,4096]{1,0:T(8,128)(2,1)} async-done(((bf16[128,4096]{1,0:T(8,128)(2,1)}), bf16[1024,4096]{1,0:T(8,128)(2,1)}) %all-gather.4.cloned.1.call-update) | async-done | bytes 8388624 | tf_op jit(solution)/shard_map/all_gather | solution.py:10
  61.9 10.7 %fusion.3 = f32[2048,1024]{0,1:T(8,128)} fusion(bf16[1024,4096]{1,0:T(8,128)(2,1)} %all-gather.4.cloned.1.call-done, bf16[1024,1024]{1,0:T(8,128)(2,1)} %param.7), kind=kOutput, calls=%fused_computation.8 | convolution fusion | flops 4299161600 | bytes 14680064 | tf_op jit(solution)/shard_map/dot_general | solution.py:49
  72.6 43.1 %all-gather.6.cloned.1.call-done = bf16[2048,1024]{1,0:T(8,128)(2,1)} async-done(((bf16[128,1024]{1,0:T(8,128)(2,1)}), bf16[2048,1024]{1,0:T(8,128)(2,1)}) %all-gather.6.cloned.1.call-update) | async-done | bytes 4194320 | tf_op jit(solution)/shard_map/all_gather | solution.py:34
  115.7 8.1 %multiply_convert_fusion.1 = bf16[1024,1024]{1,0:T(8,128)(2,1)S(1)} fusion(bf16[1024,1024]{1,0:T(8,128)(2,1)S(1)} %copy-done.1, bf16[2048,1024]{1,0:T(8,128)(2,1)} %all-gather.6.cloned.1.call-done, bf16[1024,4096]{1,0:T(8,128)(2,1)} %all-gather.4.cloned.1.call-done), kind=kOutput, calls=%fused_computation.5 | convolution fusion | flops 4300210176 | bytes 12582912 | tf_op jit(solution)/shard_map/dot_general | solution.py:32
  123.9 4.9 %fusion.1 = f32[2048,1024]{0,1:T(8,128)S(1)} fusion(bf16[1024,1024]{1,0:T(8,128)(2,1)S(1)} %multiply_convert_fusion.1, bf16[1024,4096]{1,0:T(8,128)(2,1)S(1)} %copy-done), kind=kOutput, calls=%fused_computation.2 | convolution fusion | flops 4294967296 | bytes 14680064 | tf_op jit(solution)/shard_map/dot_general | solution.py:52
  128.8 4.8 %fusion = bf16[2048,2048]{0,1:T(8,128)(2,1)} fusion(f32[2048,1024]{0,1:T(8,128)S(1)} %fusion.1, f32[2048,1024]{0,1:T(8,128)S(1)} %bitcast.7), kind=kLoop, calls=%fused_computation.1 | loop fusion | flops 12582912 | bytes 25165824 | tf_op jit(solution)/shard_map/convert_element_type | solution.py:56
  133.6 12.4 %copy.12 = bf16[2048,2048]{1,0:T(8,128)(2,1)} copy(bf16[2048,2048]{0,1:T(8,128)(2,1)} %fusion) | data formatting | bytes 16777216
  146.0 0.0 reduce-scatter.4.cloned.1.call-update
  146.0 22.9 %all-gather.8.cloned.1.call-done = bf16[2048,1024]{1,0:T(8,128)(2,1)} async-done(((bf16[128,1024]{1,0:T(8,128)(2,1)}), bf16[2048,1024]{1,0:T(8,128)(2,1)}) %all-gather.8.cloned.1.call-update) | async-done | bytes 4194320 | tf_op jit(solution)/shard_map/all_gather | solution.py:40
  169.0 6.9 %convolution_convert_fusion = bf16[1024,2048]{1,0:T(8,128)(2,1)S(1)} fusion(bf16[1024,1024]{1,0:T(8,128)(2,1)S(1)} %copy-done.3, bf16[2048,1024]{1,0:T(8,128)(2,1)} %all-gather.8.cloned.1.call-done), kind=kOutput, calls=%fused_computation.7 | convolution fusion | flops 4297064448 | bytes 10485760 | tf_op jit(solution)/shard_map/dot_general | solution.py:38
  175.9 53.9 %all_to_all.5 = bf16[8,128,2048]{2,1,0:T(8,128)(2,1)} all-to-all(bf16[8,128,2048]{2,1,0:T(8,128)(2,1)S(1)} %bitcast.8), channel_id=1, replica_groups=mesh['rep'=16,'fs'=4,'tp'=2] {'fs','tp'}, dimensions={0} | all-to-all | bytes 8388608 | tf_op jit(solution)/shard_map/all_to_all | solution.py:22
  229.8 3.9 %reduce_sum.12 = bf16[128,2048]{1,0:T(8,128)(2,1)} reduce(bf16[8,128,2048]{2,1,0:T(8,128)(2,1)} %all_to_all.5, bf16[]{:T(256)} %constant.3.clone.1), dimensions={0}, to_apply=%region_0.0 | reduce | flops 1835008 | bytes 4718594 | tf_op jit(solution)/shard_map/reduce_sum | solution.py:23
  233.6 24.1 %reduce-scatter.4.cloned.1.call-done = bf16[128,2048]{1,0:T(8,128)(2,1)} async-done(((bf16[2048,2048]{1,0:T(8,128)(2,1)}), bf16[128,2048]{1,0:T(8,128)(2,1)}) %reduce-scatter.4.cloned.1.call-update) | async-done | bytes 524304
  257.8 1.3 copy.13
  259.1 0.1 fusion.11
  259.2 1.0 copy.11
  260.2 1.0 copy.10
  (14 shorter events, 0.0 us)
Async XLA Ops:
  7.2 54.7 %all-gather.4.cloned.1.call-start = ((), (), s32[]{:S(2)}) async-start(), calls=%async_computation.2 | async-start | bytes 9437184 | tf_op jit(solution)/shard_map/all_gather | solution.py:10
  9.6 106.1 %all-gather.6.cloned.1.call-start = ((), (), s32[]{:S(2)}) async-start(), calls=%async_computation.3 | async-start | bytes 4456448 | tf_op jit(solution)/shard_map/all_gather | solution.py:34
  10.3 158.6 %all-gather.8.cloned.1.call-start = ((), (), s32[]{:S(2)}) async-start(), calls=%async_computation.4 | async-start | bytes 4456448 | tf_op jit(solution)/shard_map/all_gather | solution.py:40
  11.1 104.6 %copy-start.1 = (bf16[1024,1024]{1,0:T(8,128)(2,1)S(1)}, bf16[1024,1024]{1,0:T(8,128)(2,1)}, u32[]{:S(2)}) copy-start(bf16[1024,1024]{1,0:T(8,128)(2,1)} %param.7) | copy-start | bytes 6291460
  11.1 246.7 %reduce-scatter.4.cloned.1.call-start = ((), (), s32[]{:S(2)}) async-start(), calls=%async_computation.5 | async-start | bytes 8912896
  115.7 8.1 %copy-start = (bf16[1024,4096]{1,0:T(8,128)(2,1)S(1)}, bf16[1024,4096]{1,0:T(8,128)(2,1)}, u32[]{:S(2)}) copy-start(bf16[1024,4096]{1,0:T(8,128)(2,1)} %all-gather.4.cloned.1.call-done) | copy-start | bytes 25165828
  115.7 13.1 %slice-start = ((s8[8388608]{0:T(1024)(128)(4,1)}), s8[4194304]{0:T(1024)(128)(4,1)S(1)}, s32[]{:S(2)}) async-start(s8[8388608]{0:T(1024)(128)(4,1)} %bitcast.6), calls=%async_computation.6 | async-start | bytes 8388608
  123.8 5.0 %copy-start.2 = (bf16[1024,1024]{1,0:T(8,128)(2,1)}, bf16[1024,1024]{1,0:T(8,128)(2,1)S(1)}, u32[]{:S(2)}) copy-start(bf16[1024,1024]{1,0:T(8,128)(2,1)S(1)} %multiply_convert_fusion.1) | copy-start | bytes 6291460
  123.8 5.0 %slice-start.1 = ((s8[8388608]{0:T(1024)(128)(4,1)}), s8[4194304]{0:T(1024)(128)(4,1)S(1)}, s32[]{:S(2)}) async-start(s8[8388608]{0:T(1024)(128)(4,1)} %bitcast.6), calls=%async_computation.7 | async-start | bytes 8388608
  146.0 23.0 %copy-start.3 = (bf16[1024,1024]{1,0:T(8,128)(2,1)S(1)}, bf16[1024,1024]{1,0:T(8,128)(2,1)}, u32[]{:S(2)}) copy-start(bf16[1024,1024]{1,0:T(8,128)(2,1)} %copy-done.2) | copy-start | bytes 6291460
Sparse Core Ops, SparseCore 0:
  9.7 52.1 all-gather.3
  64.0 51.6 all-gather.5
  117.9 51.0 all-gather.7
  172.2 85.5 reduce-scatter.3
where the time goes:
time: 268 us
  waiting for transfers between devices  142 us (53%)
  blocking collectives  53.9 us (20%)
  matrix products  30.7 us (11%)
  local copies, waits for them, and re-layouts  15.8 us (6%)
  between operations  13.9 us (5%)
  other arithmetic  11 us (4%)
    all_to_all x1, blocking collectives, sent_and_summed(): lax.all_to_all(tiles, axis, split_axis=0, concat_axis=0, tiled=True)  53.9 us
    all_gather x1, waiting for transfers between devices, side_by_side(): out = lax.all_gather(both, axis, axis=dim, tiled=True)  50.8 us
    all_gather x1, waiting for transfers between devices, on_device(): lax.all_gather(w_down_t, 'rep', axis=0, tiled=True)  43.1 us
    unnamed x5, waiting for transfers between devices  25.6 us
    all_gather x1, waiting for transfers between devices, on_device(): lax.all_gather(w_up, 'rep', axis=0, tiled=True)  22.9 us
    unnamed x16, local copies, waits for them, and re-layouts  15.7 us
    dot_general x1, matrix products, on_device(): lax.dot_general(grad_rows, squared, (((0,), (0,)), ((), ())), preferred_e...  10.7 us
    dot_general x1, matrix products, on_device(): jnp.dot(grad_rows, lax.all_gather(w_down_t, 'rep', axis=0, tiled=True), p...  8.1 us
  transfers between devices with their start and end apart: 4, of which 4 were waited for; matrix products, arithmetic and copies ran while one was open for 19% of the time, Pallas kernels for 0%

commit v1 on v0

--- a/solution.py
+++ b/solution.py
@@ -2,6 +2,17 @@
 import jax.numpy as jnp
 from jax import lax
 from jax.sharding import PartitionSpec as P
+
+
+def wait_widths(x_in):
+    link_axis = "rep"
+    lanes = jax.lax.axis_size(link_axis)
+    ledger = []
+    for w in range(x_in.ndim):
+        ledger.append(lanes if w == 0 else 1)
+    return jax.lax.all_to_all(
+        jnp.tile(x_in, ledger), link_axis, split_axis=0, concat_axis=0, tiled=True
+    )
 
 
 def side_by_side(arrays, axis, dim, along):
@@ -36,10 +47,7 @@
     )
     grad_pre = (grad_squared * 2.0 * linear).astype(jnp.bfloat16)
     partial_terms = lax.dot_general(
-        grad_pre,
-        lax.all_gather(w_up, "rep", axis=0, tiled=True),
-        (((1,), (1,)), ((), ())),
-        preferred_element_type=jnp.float32,
+        grad_pre, wait_widths(w_up), (((1,), (1,)), ((), ())), preferred_element_type=jnp.float32
     ).astype(jnp.bfloat16)
     grad_in = sent_and_summed(
         partial_terms.astype(jnp.float32).astype(jnp.bfloat16), ("fs", "tp"), 0

time: 268 us -> 293 us (1.093)
  blocking collectives: 53.9 us -> 126 us
  waiting for transfers between devices: 142 us -> 95.4 us
    all_to_all x0 -> x1, blocking collectives: none -> 71.4 us  [wait_widths(): jax.lax.all_to_all(jnp.tile(x_in, ledger), link_axis, split_axis=0, conca...]
    unnamed x5 -> x4, waiting for transfers between devices: 25.6 us -> 0.73 us
    all_gather x1 -> x0, waiting for transfers between devices: 22.9 us -> none  [on_device(): lax.all_gather(w_up, 'rep', axis=0, tiled=True)]
    unnamed x16 -> x18, local copies, waits for them, and re-layouts: 15.7 us -> 16.6 us
  transfers between devices with their start and end apart: 4 -> 3, of which waited for: 4 -> 2; matrix products, arithmetic and copies ran while one was open for 19% -> 7% of each run, Pallas kernels for 0% -> 0%
where the time goes in v1:
time: 293 us; the launch traced here: 292 us
  blocking collectives  126 us (43%)
  waiting for transfers between devices  95.4 us (33%)
  matrix products  28.5 us (10%)
  local copies, waits for them, and re-layouts  17.2 us (6%)
  between operations  13.9 us (5%)
  other arithmetic  11 us (4%)
    all_to_all x1, blocking collectives, wait_widths(): jax.lax.all_to_all(jnp.tile(x_in, ledger), link_axis, split_axis=0, conca...  71.4 us
    all_to_all x1, blocking collectives, sent_and_summed(): lax.all_to_all(tiles, axis, split_axis=0, concat_axis=0, tiled=True)  54.3 us
    all_gather x1, waiting for transfers between devices, side_by_side(): out = lax.all_gather(both, axis, axis=dim, tiled=True)  51.5 us
    all_gather x1, waiting for transfers between devices, on_device(): lax.all_gather(w_down_t, 'rep', axis=0, tiled=True)  43.2 us
    unnamed x18, local copies, waits for them, and re-layouts  16.6 us
    dot_general x1, matrix products, on_device(): lax.dot_general(grad_rows, squared, (((0,), (0,)), ((), ())), preferred_e...  10.7 us
    dot_general x1, matrix products, on_device(): jnp.dot(grad_rows, lax.all_gather(w_down_t, 'rep', axis=0, tiled=True), p...  8.09 us
  transfers between devices with their start and end apart: 3, of which 2 were waited for; matrix products, arithmetic and copies ran while one was open for 7% of the time, Pallas kernels for 0%

profile of v1, /device:TPU:0, one launch (start us, length us, event | category | flops | bytes accessed | tf_op | source)
XLA Modules:
  0.0 291.6 jit_solution(18262853683539552296)
XLA Ops:
  7.2 0.0 all-gather.3.cloned.1.call-start
  7.2 2.4 pad_maximum_fusion
  9.6 0.0 all-gather.3.cloned.1.call-update
  9.6 0.0 all-gather.5.cloned.1.call-start
  9.6 0.7 all-gather.5.cloned.1.call-update
  10.4 0.0 reduce-scatter.4.cloned.1.call-start
  10.4 51.5 %all-gather.3.cloned.1.call-done = bf16[1024,4096]{1,0:T(8,128)(2,1)} async-done(((bf16[128,4096]{1,0:T(8,128)(2,1)}), bf16[1024,4096]{1,0:T(8,128)(2,1)}) %all-gather.3.cloned.1.call-update) | async-done | bytes 8388624 | tf_op jit(solution)/shard_map/all_gather | solution.py:21
  61.9 10.7 %fusion.3 = f32[2048,1024]{0,1:T(8,128)} fusion(bf16[1024,4096]{1,0:T(8,128)(2,1)} %all-gather.3.cloned.1.call-done, bf16[1024,1024]{1,0:T(8,128)(2,1)} %param.7), kind=kOutput, calls=%fused_computation.8 | convolution fusion | flops 4299161600 | bytes 14680064 | tf_op jit(solution)/shard_map/dot_general | solution.py:57
  72.6 43.2 %all-gather.5.cloned.1.call-done = bf16[2048,1024]{1,0:T(8,128)(2,1)} async-done(((bf16[128,1024]{1,0:T(8,128)(2,1)}), bf16[2048,1024]{1,0:T(8,128)(2,1)}) %all-gather.5.cloned.1.call-update) | async-done | bytes 4194320 | tf_op jit(solution)/shard_map/all_gather | solution.py:45
  115.7 8.1 %multiply_convert_fusion.1 = bf16[1024,1024]{1,0:T(8,128)(2,1)S(1)} fusion(bf16[1024,1024]{1,0:T(8,128)(2,1)S(1)} %copy-done.2, bf16[2048,1024]{1,0:T(8,128)(2,1)} %all-gather.5.cloned.1.call-done, bf16[1024,4096]{1,0:T(8,128)(2,1)} %all-gather.3.cloned.1.call-done), kind=kOutput, calls=%fused_computation.5 | convolution fusion | flops 4300210176 | bytes 12582912 | tf_op jit(solution)/shard_map/dot_general | solution.py:43
  123.9 4.9 %fusion.1 = f32[2048,1024]{0,1:T(8,128)S(1)} fusion(bf16[1024,1024]{1,0:T(8,128)(2,1)S(1)} %multiply_convert_fusion.1, bf16[1024,4096]{1,0:T(8,128)(2,1)S(1)} %copy-done.1), kind=kOutput, calls=%fused_computation.2 | convolution fusion | flops 4294967296 | bytes 14680064 | tf_op jit(solution)/shard_map/dot_general | solution.py:60
  128.9 4.8 %fusion = bf16[2048,2048]{0,1:T(8,128)(2,1)} fusion(f32[2048,1024]{0,1:T(8,128)S(1)} %fusion.1, f32[2048,1024]{0,1:T(8,128)S(1)} %bitcast.8), kind=kLoop, calls=%fused_computation.1 | loop fusion | flops 12582912 | bytes 25165824 | tf_op jit(solution)/shard_map/convert_element_type | solution.py:64
  133.6 12.3 %copy.12 = bf16[2048,2048]{1,0:T(8,128)(2,1)} copy(bf16[2048,2048]{0,1:T(8,128)(2,1)} %fusion) | data formatting | bytes 16777216
  145.9 0.0 reduce-scatter.4.cloned.1.call-update
  146.0 0.9 copy-done
  146.9 0.5 tile.2
  147.4 71.4 %all_to_all.14 = bf16[16,128,1024]{2,1,0:T(8,128)(2,1)S(1)} all-to-all(bf16[16,128,1024]{2,1,0:T(8,128)(2,1)S(1)} %tile.2), channel_id=1, replica_groups=mesh['rep'=16,'fs'=4,'tp'=2] {'rep'}, dimensions={0} | all-to-all | bytes 8388608 | tf_op jit(solution)/shard_map/all_to_all | solution.py:13
  218.8 4.8 %convolution_convert_fusion = bf16[1024,2048]{1,0:T(8,128)(2,1)S(1)} fusion(bf16[1024,1024]{1,0:T(8,128)(2,1)S(1)} %copy-done.4, bf16[2048,1024]{1,0:T(8,128)(2,1)S(1)} %bitcast.9), kind=kOutput, calls=%fused_computation.7 | convolution fusion | flops 4297064448 | bytes 10485760 | tf_op jit(solution)/shard_map/dot_general | solution.py:49
  223.6 54.3 %all_to_all.15 = bf16[8,128,2048]{2,1,0:T(8,128)(2,1)} all-to-all(bf16[8,128,2048]{2,1,0:T(8,128)(2,1)S(1)} %bitcast.10), channel_id=1, replica_groups=mesh['rep'=16,'fs'=4,'tp'=2] {'fs','tp'}, dimensions={0} | all-to-all | bytes 8388608 | tf_op jit(solution)/shard_map/all_to_all | solution.py:33
  277.9 3.8 %reduce_sum.12 = bf16[128,2048]{1,0:T(8,128)(2,1)} reduce(bf16[8,128,2048]{2,1,0:T(8,128)(2,1)} %all_to_all.15, bf16[]{:T(256)} %constant.3.clone.1), dimensions={0}, to_apply=%region_0.0 | reduce | flops 1835008 | bytes 4718594 | tf_op jit(solution)/shard_map/reduce_sum | solution.py:34
  281.7 1.3 copy.13
  283.0 0.1 fusion.11
  283.1 1.0 copy.11
  284.1 1.0 copy.10
  (15 shorter events, 0.0 us)
Async XLA Ops:
  7.2 54.7 %all-gather.3.cloned.1.call-start = ((), (), s32[]{:S(2)}) async-start(), calls=%async_computation.3 | async-start | bytes 9437184 | tf_op jit(solution)/shard_map/all_gather | solution.py:21
  9.6 106.1 %all-gather.5.cloned.1.call-start = ((), (), s32[]{:S(2)}) async-start(), calls=%async_computation.4 | async-start | bytes 4456448 | tf_op jit(solution)/shard_map/all_gather | solution.py:45
  10.4 105.4 %copy-start.2 = (bf16[1024,1024]{1,0:T(8,128)(2,1)S(1)}, bf16[1024,1024]{1,0:T(8,128)(2,1)}, u32[]{:S(2)}) copy-start(bf16[1024,1024]{1,0:T(8,128)(2,1)} %param.7) | copy-start | bytes 6291460
  10.4 271.4 %reduce-scatter.4.cloned.1.call-start = ((), (), s32[]{:S(2)}) async-start(), calls=%async_computation.5 | async-start | bytes 8912896
  115.7 8.1 %copy-start.1 = (bf16[1024,4096]{1,0:T(8,128)(2,1)S(1)}, bf16[1024,4096]{1,0:T(8,128)(2,1)}, u32[]{:S(2)}) copy-start(bf16[1024,4096]{1,0:T(8,128)(2,1)} %all-gather.3.cloned.1.call-done) | copy-start | bytes 25165828
  115.7 13.1 %slice-start = ((s8[8388608]{0:T(1024)(128)(4,1)}), s8[4194304]{0:T(1024)(128)(4,1)S(1)}, s32[]{:S(2)}) async-start(s8[8388608]{0:T(1024)(128)(4,1)} %bitcast.7), calls=%async_computation.6 | async-start | bytes 8388608
  123.8 5.0 %copy-start.3 = (bf16[1024,1024]{1,0:T(8,128)(2,1)}, bf16[1024,1024]{1,0:T(8,128)(2,1)S(1)}, u32[]{:S(2)}) copy-start(bf16[1024,1024]{1,0:T(8,128)(2,1)S(1)} %multiply_convert_fusion.1) | copy-start | bytes 6291460
  123.9 5.0 %slice-start.1 = ((s8[8388608]{0:T(1024)(128)(4,1)}), s8[4194304]{0:T(1024)(128)(4,1)S(1)}, s32[]{:S(2)}) async-start(s8[8388608]{0:T(1024)(128)(4,1)} %bitcast.7), calls=%async_computation.7 | async-start | bytes 8388608
  145.9 0.9 copy-start
  147.4 71.4 %copy-start.4 = (bf16[1024,1024]{1,0:T(8,128)(2,1)S(1)}, bf16[1024,1024]{1,0:T(8,128)(2,1)}, u32[]{:S(2)}) copy-start(bf16[1024,1024]{1,0:T(8,128)(2,1)} %copy-done.3) | copy-start | bytes 6291460
Sparse Core Ops, SparseCore 0:
  9.7 52.1 all-gather.2
  64.1 51.6 all-gather.4
  146.1 121.6 reduce-scatter.3
